TPU v7x, 512 devices: a 4x2x32 block of a 4x8x32 slice. The times are simulated.
512 devices in a mesh: grp: 2 (over y), ep: 64 (over z, core), tp: 4 (over x).
Axes of the slice: x: 4, y: 2, z: 32, core: 2. Of those that a mesh axis runs over, the one named last changes fastest.
The devices are a block of a 4x8x32 slice.
Arguments:
- tokens: bfloat16 [49152, 2048], P(('grp', 'ep'), 'tp'), parts along dimension 0
- group_choice: int32 [49152], P(('grp', 'ep')), parts along dimension 0, may hold values from 0 to 7, as said below
- expert_choice: int32 [49152, 2], P(('grp', 'ep')), parts along dimension 0, may hold values from 0 to 7, as said below
- group_weight: float32 [49152], P(('grp', 'ep')), parts along dimension 0, may hold values from 0.3 to 1
- expert_weight: float32 [49152, 2], P(('grp', 'ep')), parts along dimension 0, may hold values from 0.1 to 1
- norm_gain: float32 [2048], replicated, may hold values from 0.1 to 1.9
- w_gate: bfloat16 [64, 2048, 1024], P('ep', None, 'tp'), may hold values from -0.125 to 0.125
- w_up: bfloat16 [64, 2048, 1024], P('ep', None, 'tp'), may hold values from -0.125 to 0.125
- w_down: bfloat16 [64, 1024, 2048], P('ep', None, 'tp'), may hold values from -0.1875 to 0.1875
Outputs:
- moe_out: bfloat16 [49152, 2048], P(('grp', 'ep'), 'tp'), parts along dimension 0
There are 2 independent parts, one for each index of `grp`. A program takes and returns all parts, laid end to end along the dimension named above; an argument that names none is the same for every part. Nothing has to cross between parts.
Inputs may be any that keep to these rules, and one draw needn't show every extreme that they name: `group_choice`: group of each token, 0 to 7; within each aligned block of 384 tokens (the tokens of one index of ep) every group is chosen by the same number of tokens. `expert_choice`: a token's two entries differ; within each aligned block of 384 tokens no expert (group with entry) is named by more than 18 tokens, and in every block one expert of each group, the same one in all blocks, is named by exactly 18 tokens.
All inputs are finite; a program needn't handle non-finite values.
Results may differ from a plain program's by a relative error of at most 0.0071.
Values may be sent and summed in bfloat16 or wider, within the bound.
A program may use at most 64 MiB of HBM per device.

v0:
```python
import jax
import jax.numpy as jnp
from jax import lax
from jax.sharding import Mesh
from jax.sharding import PartitionSpec as P

EP = ("ep_0", "ep_1")
GRP_EP = ("grp", "ep_0", "ep_1")


def copy_for_each(array, axis):
    length = lax.axis_size(axis)
    return lax.all_to_all(
        jnp.broadcast_to(array[None], (length, *array.shape)), axis, 0, 0, tiled=True
    )


def laid_out(blocks, dim):
    dims = list(blocks.shape[1:])
    dims[dim] *= blocks.shape[0]
    return jnp.moveaxis(blocks, 0, dim).reshape(dims)


def collect(array, axis, dim):
    blocks = copy_for_each(array, axis)
    return laid_out(blocks, dim)


def over_copies(array, axis):
    everything = copy_for_each(array, axis)
    return jnp.sum(everything, axis=0)


def cut_along(array, dim, length):
    dims = array.shape
    blocks = array.reshape(*dims[:dim], length, dims[dim] // length, *dims[dim + 1 :])
    return jnp.moveaxis(blocks, dim, 0)


def moved_by_axis(blocks, axes, turns):
    dims = [lax.axis_size(a) for a in axes]
    blocks = blocks.reshape(*dims, *blocks.shape[1:])
    for k in turns:
        blocks = lax.all_to_all(blocks, axes[k], split_axis=k, concat_axis=k, tiled=True)
    return blocks.reshape(-1, *blocks.shape[len(axes) :])


def exchange_by_chip(array, groups, turns, split_dim, concat_dim):
    length = lax.axis_size(groups[0]) * lax.axis_size(groups[1])
    blocks = cut_along(array, split_dim, length)
    return laid_out(moved_by_axis(blocks, groups, turns), concat_dim)


def finish_rows(gate_sum, up_sum, w_down):
    hidden = (jax.nn.silu(gate_sum) * up_sum).astype(jnp.bfloat16)
    whole_hidden = collect(hidden, "tp", 3)
    summed = jnp.einsum("sxcf,xfd->sxcd", whole_hidden, w_down, preferred_element_type=jnp.float32)
    return summed.astype(jnp.bfloat16)


def body(
    tokens,
    group_choice,
    expert_choice,
    group_weight,
    expert_weight,
    norm_gain,
    w_gate,
    w_up,
    w_down,
):
    tok_rows = tokens.shape[0]
    ep_count = lax.axis_size(EP)
    exp_local = w_gate.shape[0]
    experts_all = ep_count * exp_local
    group_size = min(8, experts_all // 2)
    group_count = experts_all // group_size
    mean_load = 2 * tok_rows // experts_all
    capacity = mean_load + min(mean_load // 2, tok_rows // group_count - mean_load)
    model_width = norm_gain.shape[0]
    expert_ids = group_choice[:, None] * group_size + expert_choice
    mixing = group_weight[:, None] * expert_weight / jnp.sum(expert_weight, -1, keepdims=True)
    flat_ids = expert_ids.reshape(-1)
    marks = (flat_ids[:, None] == jnp.arange(experts_all, dtype=jnp.int32)[None, :]).astype(
        jnp.int32
    )
    earlier = jnp.cumsum(marks, 0) - marks
    seat_index = jnp.sum(earlier * marks, 1)
    targets = (flat_ids * capacity + seat_index).reshape(tok_rows, 2)
    places = jnp.arange(experts_all * capacity, dtype=jnp.int32)
    dispatch = (
        (places[:, None] == targets[None, :, 0]) | (places[:, None] == targets[None, :, 1])
    ).astype(jnp.bfloat16)
    values = tokens.astype(jnp.float32)
    own_squares = jnp.sum(values * values, -1)
    all_squares = over_copies(own_squares, "tp")
    inv_rms = lax.rsqrt(all_squares / model_width + 1e-06)
    piece_width = tokens.shape[1]
    gain_piece = lax.dynamic_slice_in_dim(
        norm_gain, lax.axis_index("tp") * piece_width, piece_width, 0
    )
    normed = (values * inv_rms[:, None] * gain_piece[None, :]).astype(jnp.bfloat16)
    buffer = jnp.dot(dispatch, normed, preferred_element_type=jnp.float32).astype(jnp.bfloat16)
    buffer = buffer.reshape(ep_count, exp_local, capacity, piece_width)
    piece = lax.all_gather(
        lax.all_to_all(buffer, EP, split_axis=0, concat_axis=0, tiled=True),
        "tp",
        axis=3,
        tiled=True,
    )
    gate_next = jnp.einsum("sxcd,xdf->sxcf", piece, w_gate, preferred_element_type=jnp.float32)
    up_next = jnp.einsum("sxcd,xdf->sxcf", piece, w_up, preferred_element_type=jnp.float32)
    results = finish_rows(gate_next, up_next, w_down)
    returned = exchange_by_chip(results, ("ep_0", "ep_1"), (1, 0), 0, 0)
    returned = returned.reshape(experts_all * capacity, returned.shape[3])
    combined = jnp.zeros((tok_rows, returned.shape[1]), jnp.float32)
    for choice_index in range(2):
        picker = (targets[:, choice_index : choice_index + 1] == places[None, :]).astype(
            jnp.bfloat16
        )
        picked = jnp.dot(picker, returned, preferred_element_type=jnp.float32)
        combined = combined + mixing[:, choice_index : choice_index + 1] * picked
    return combined.astype(jnp.bfloat16)


def solution(mesh):
    split = Mesh(
        mesh.devices.reshape(mesh.shape["grp"], 32, 2, mesh.shape["tp"]),
        ("grp", "ep_0", "ep_1", "tp"),
    )
    placed = (
        P(GRP_EP, "tp"),
        P(GRP_EP),
        P(GRP_EP, None),
        P(GRP_EP),
        P(GRP_EP, None),
        P(),
        P(EP, None, "tp"),
        P(EP, None, "tp"),
        P(EP, None, "tp"),
    )
    return jax.shard_map(
        body, mesh=split, in_specs=placed, out_specs=P(GRP_EP, "tp"), check_vma=False
    )
```

profile of v0, /device:TPU:33, one launch (start us, length us, event | category | flops | bytes accessed | tf_op | source)
XLA Modules:
  0.0 482.4 jit_solution(356377158643691526)
XLA Ops:
  6.6 1.2 fusion.35
  8.4 5.1 %all-to-all-start = ((f32[4,1,384]{2,1,0:T(1,128)}), f32[4,1,384]{2,1,0:T(1,128)S(1)}, u32[]{:S(2)}, u32[]{:S(2)}) async-start(f32[4,1,384]{2,1,0:T(1,128)} %broadcast_in_dim.6), calls=%async_computation | async-start | bytes 12288 | tf_op jit(solution)/shard_map/all_to_all | solution.py:13
  13.5 0.8 copy.35
  15.5 1.8 reduce-window.6
  18.3 0.8 dynamic_slice.3
  19.1 1.9 convolution_convert_fusion
  21.0 2.2 reshape.67
  23.2 199.5 %all_to_all.26 = bf16[64,1,18,512]{3,2,1,0:T(8,128)(2,1)S(1)} all-to-all(bf16[64,1,18,512]{3,2,1,0:T(8,128)(2,1)S(1)} %bitcast.87), channel_id=1, replica_groups=mesh['grp'=2,'ep_0'=32,'ep_1'=2,'tp'=4] {'ep_0','ep_1'}, dimensions={0} | all-to-all | bytes 2359296 | tf_op jit(solution)/shard_map/all_to_all | solution.py:106
  222.7 1.4 copy.39
  224.2 52.9 %all-gather.2.cloned.1.call-done = bf16[64,1,18,2048]{3,0,2,1:T(8,128)(2,1)} async-done(((bf16[64,1,18,512]{3,0,2,1:T(8,128)(2,1)}), bf16[64,1,18,2048]{3,0,2,1:T(8,128)(2,1)}) %all-gather.2.cloned.1.call-update) | async-done | bytes 4718608 | tf_op jit(solution)/shard_map/all_gather | solution.py:105
  277.1 3.9 fusion.9
  281.0 1.5 fusion.25
  282.8 31.1 %all_to_all.27 = bf16[4,64,1,18,256]{4,1,3,2,0:T(8,128)(2,1)S(1)} all-to-all(bf16[4,64,1,18,256]{4,1,3,2,0:T(8,128)(2,1)S(1)} %broadcast_in_dim.8), channel_id=1, replica_groups=mesh['grp'=2,'ep_0'=32,'ep_1'=2,'tp'=4] {'tp'}, dimensions={0} | all-to-all | bytes 4718592 | tf_op jit(solution)/shard_map/all_to_all | solution.py:13
  313.9 2.0 copy.40
  315.9 2.9 reshape.71
  318.8 3.0 fusion.8
  322.6 6.3 %all_to_all.28 = bf16[32,2,1,1,18,512]{5,0,4,3,2,1:T(8,128)(2,1)S(1)} all-to-all(bf16[32,2,1,1,18,512]{5,0,4,3,2,1:T(8,128)(2,1)S(1)} %copy.41), channel_id=1, replica_groups=mesh['grp'=2,'ep_0'=32,'ep_1'=2,'tp'=4] {'ep_1'}, dimensions={1} | all-to-all | bytes 2359296 | tf_op jit(solution)/shard_map/all_to_all | solution.py:44
  328.9 2.3 copy.42
  331.2 23.3 %all-to-all-start.4 = ((bf16[32,2,1,1,18,512]{5,1,4,3,2,0:T(2,128)(2,1)}), bf16[32,2,1,1,18,512]{5,1,4,3,2,0:T(2,128)(2,1)}, u32[]{:S(2)}, u32[]{:S(2)}) async-start(bf16[32,2,1,1,18,512]{5,1,4,3,2,0:T(2,128)(2,1)} %copy.42), calls=%async_computation.4 | async-start | bytes 2359296 | tf_op jit(solution)/shard_map/all_to_all | solution.py:44
  354.6 114.5 %all-to-all-done.4 = bf16[32,2,1,1,18,512]{5,1,4,3,2,0:T(2,128)(2,1)} async-done(((bf16[32,2,1,1,18,512]{5,1,4,3,2,0:T(2,128)(2,1)}), bf16[32,2,1,1,18,512]{5,1,4,3,2,0:T(2,128)(2,1)}, u32[]{:S(2)}, u32[]{:S(2)}) %all-to-all-start.4) | async-done | bytes 1179680 | tf_op jit(solution)/shard_map/all_to_all | solution.py:44
  469.1 1.6 copy.43
  470.7 1.2 reshape_reshape_reshape.3
  472.0 2.1 fusion.23
  474.0 1.5 fusion.24
  (39 shorter events, 3.9 us)
Async XLA Ops:
  6.5 312.3 %copy-start = (bf16[1,1024,512]{2,1,0:T(8,128)(2,1)S(1)}, bf16[1,1024,512]{2,1,0:T(8,128)(2,1)}, u32[]{:S(2)}) copy-start(bf16[1,1024,512]{2,1,0:T(8,128)(2,1)} %param.17) | copy-start | bytes 3145732
  8.4 10.6 %all-to-all-start = ((f32[4,1,384]{2,1,0:T(1,128)}), f32[4,1,384]{2,1,0:T(1,128)S(1)}, u32[]{:S(2)}, u32[]{:S(2)}) async-start(f32[4,1,384]{2,1,0:T(1,128)} %broadcast_in_dim.6), calls=%async_computation | async-start | bytes 12288 | tf_op jit(solution)/shard_map/all_to_all | solution.py:13
  13.5 263.6 %all-gather.2.cloned.1.call-start = ((), (), s32[]{:S(2)}) async-start(), calls=%async_computation.5 | async-start | bytes 5898240 | tf_op jit(solution)/shard_map/all_gather | solution.py:105
  15.3 3.8 copy-start.2
  224.1 53.0 %copy-start.6 = (bf16[1,2048,256]{2,1,0:T(8,128)(2,1)S(1)}, bf16[1,2048,256]{2,1,0:T(8,128)(2,1)}, u32[]{:S(2)}) copy-start(bf16[1,2048,256]{2,1,0:T(8,128)(2,1)} %param.15) | copy-start | bytes 3145732
  224.2 56.8 %copy-start.7 = (bf16[1,2048,256]{2,1,0:T(8,128)(2,1)S(1)}, bf16[1,2048,256]{2,1,0:T(8,128)(2,1)}, u32[]{:S(2)}) copy-start(bf16[1,2048,256]{2,1,0:T(8,128)(2,1)} %param.16) | copy-start | bytes 3145732
  277.1 3.9 copy-start.5
  331.2 23.4 %copy-start.3 = (f32[384,2]{0,1:T(2,128)S(1)}, f32[384,2]{0,1:T(2,128)}, u32[]{:S(2)}) copy-start(f32[384,2]{0,1:T(2,128)} %param.13) | copy-start | bytes 9220
  331.2 23.4 %copy-start.4 = (f32[384]{0:T(512)S(1)}, f32[384]{0:T(512)}, u32[]{:S(2)}) copy-start(f32[384]{0:T(512)} %param.12) | copy-start | bytes 4612
  331.2 137.9 %all-to-all-start.4 = ((bf16[32,2,1,1,18,512]{5,1,4,3,2,0:T(2,128)(2,1)}), bf16[32,2,1,1,18,512]{5,1,4,3,2,0:T(2,128)(2,1)}, u32[]{:S(2)}, u32[]{:S(2)}) async-start(bf16[32,2,1,1,18,512]{5,1,4,3,2,0:T(2,128)(2,1)} %copy.42), calls=%async_computation.4 | async-start | bytes 2359296 | tf_op jit(solution)/shard_map/all_to_all | solution.py:44
  472.0 2.1 copy-start.1
Sparse Core Ops, SparseCore 0:
  224.3 52.7 all-gather.1
where the time goes:
time: 483 us; the launch traced here: 482 us
  blocking collectives  237 us (49%)
  waiting for transfers between devices  167 us (35%)
  starting transfers between devices  28.5 us (6%)
  local copies, waits for them, and re-layouts  17.8 us (4%)
  matrix products  13.9 us (3%)
  between operations  13.6 us (3%)
    all_to_all x1, blocking collectives, body(): lax.all_to_all(buffer, EP, split_axis=0, concat_axis=0, tiled=True)  200 us
    all_to_all x1, waiting for transfers between devices, moved_by_axis(): lax.all_to_all(blocks, axes[k], split_axis=k, concat_axis=k, tiled=True)  115 us
    all_gather x1, waiting for transfers between devices, body(): lax.all_gather(lax.all_to_all(buffer, EP, split_axis=0, concat_axis=0, ti...  52.9 us
    all_to_all x1, blocking collectives, copy_for_each(): lax.all_to_all(jnp.broadcast_to(array[None], (length, *array.shape)), axi...  31.1 us
    all_to_all x1, starting transfers between devices, moved_by_axis(): lax.all_to_all(blocks, axes[k], split_axis=k, concat_axis=k, tiled=True)  23.3 us
  transfers between devices with their start and end apart: 3, of which 2 were waited for; matrix products, arithmetic and copies ran while one was open for 1% of the time, Pallas kernels for 0%

commit v1 on v0

--- a/solution.py
+++ b/solution.py
@@ -6,6 +6,12 @@
 
 EP = ("ep_0", "ep_1")
 GRP_EP = ("grp", "ep_0", "ep_1")
+
+
+def gather_by_exchange(x, axis, dim):
+    size = lax.axis_size(axis)
+    repeats = [size if d == dim else 1 for d in range(x.ndim)]
+    return lax.all_to_all(jnp.tile(x, repeats), axis, split_axis=dim, concat_axis=dim, tiled=True)
 
 
 def copy_for_each(array, axis):
@@ -102,11 +108,8 @@
     normed = (values * inv_rms[:, None] * gain_piece[None, :]).astype(jnp.bfloat16)
     buffer = jnp.dot(dispatch, normed, preferred_element_type=jnp.float32).astype(jnp.bfloat16)
     buffer = buffer.reshape(ep_count, exp_local, capacity, piece_width)
-    piece = lax.all_gather(
-        lax.all_to_all(buffer, EP, split_axis=0, concat_axis=0, tiled=True),
-        "tp",
-        axis=3,
-        tiled=True,
+    piece = gather_by_exchange(
+        lax.all_to_all(buffer, EP, split_axis=0, concat_axis=0, tiled=True), "tp", 3
     )
     gate_next = jnp.einsum("sxcd,xdf->sxcf", piece, w_gate, preferred_element_type=jnp.float32)
     up_next = jnp.einsum("sxcd,xdf->sxcf", piece, w_up, preferred_element_type=jnp.float32)

time: 483 us -> 508 us (1.052)
  blocking collectives: 237 us -> 295 us
  waiting for transfers between devices: 167 us -> 115 us
  local copies, waits for them, and re-layouts: 17.8 us -> 66.3 us
  starting transfers between devices: 28.5 us -> 12.3 us
  between operations: 13.6 us -> 0.21 us
    all_to_all x0 -> x1, blocking collectives: none -> 58.6 us  [gather_by_exchange(): lax.all_to_all(jnp.tile(x, repeats), axis, split_axis=dim, concat_axis=di...]
    all_gather x1 -> x0, waiting for transfers between devices: 52.9 us -> none  [body(): lax.all_gather(lax.all_to_all(buffer, EP, split_axis=0, concat_axis=0, ti...]
    unnamed x17 -> x19, local copies, waits for them, and re-layouts: 0.85 us -> 23.1 us
    all_to_all x1, starting transfers between devices: 23.3 us -> 7.16 us  [moved_by_axis(): lax.all_to_all(blocks, axes[k], split_axis=k, concat_axis=k, tiled=True)]
    another operation x1 -> x3, local copies, waits for them, and re-layouts: 2.9 us -> 16.7 us  [the longest x2 13.7 us: gather_by_exchange(): jnp.tile(x, repeats)]
    all_to_all x1, local copies, waits for them, and re-layouts: 1.42 us -> 13.9 us  [gather_by_exchange(): lax.all_to_all(jnp.tile(x, repeats), axis, split_axis=dim, concat_axis=di...]
  transfers between devices with their start and end apart: 3 -> 2, of which waited for: 2 -> 1; matrix products, arithmetic and copies ran while one was open for 1% -> 1% of each run, Pallas kernels for 0% -> 0%
where the time goes in v1:
time: 508 us; the launch traced here: 507 us
  blocking collectives  295 us (58%)
  waiting for transfers between devices  115 us (23%)
  local copies, waits for them, and re-layouts  66.3 us (13%)
  matrix products  13.9 us (3%)
  starting transfers between devices  12.3 us (2%)
    all_to_all x1, blocking collectives, body(): lax.all_to_all(buffer, EP, split_axis=0, concat_axis=0, tiled=True)  200 us
    all_to_all x1, waiting for transfers between devices, moved_by_axis(): lax.all_to_all(blocks, axes[k], split_axis=k, concat_axis=k, tiled=True)  115 us
    all_to_all x1, blocking collectives, gather_by_exchange(): lax.all_to_all(jnp.tile(x, repeats), axis, split_axis=dim, concat_axis=di...  58.6 us
    all_to_all x1, blocking collectives, copy_for_each(): lax.all_to_all(jnp.broadcast_to(array[None], (length, *array.shape)), axi...  28.5 us
    unnamed x19, local copies, waits for them, and re-layouts  23.1 us
    all_to_all x1, local copies, waits for them, and re-layouts, gather_by_exchange(): lax.all_to_all(jnp.tile(x, repeats), axis, split_axis=dim, concat_axis=di...  13.9 us
    another operation x2, local copies, waits for them, and re-layouts, gather_by_exchange(): jnp.tile(x, repeats)  13.7 us
  transfers between devices with their start and end apart: 2, of which 1 were waited for; matrix products, arithmetic and copies ran while one was open for 1% of the time, Pallas kernels for 0%

profile of v1, /device:TPU:33, one launch (start us, length us, event | category | flops | bytes accessed | tf_op | source)
XLA Modules:
  0.0 506.6 jit_solution(6576323291717632172)
XLA Ops:
  1.8 5.1 %all-to-all-start = ((f32[4,1,384]{2,1,0:T(1,128)}), f32[4,1,384]{2,1,0:T(1,128)S(1)}, u32[]{:S(2)}, u32[]{:S(2)}) async-start(f32[4,1,384]{2,1,0:T(1,128)} %broadcast_in_dim.6), calls=%async_computation | async-start | bytes 12288 | tf_op jit(solution)/shard_map/all_to_all | solution.py:19
  9.0 1.8 reduce-window.6
  12.6 1.9 convolution_convert_fusion
  14.5 2.2 reshape.73
  16.7 199.6 %all_to_all.31 = bf16[64,1,18,512]{3,2,1,0:T(8,128)(2,1)} all-to-all(bf16[64,1,18,512]{3,2,1,0:T(8,128)(2,1)S(1)} %bitcast.93), channel_id=1, replica_groups=mesh['grp'=2,'ep_0'=32,'ep_1'=2,'tp'=4] {'ep_0','ep_1'}, dimensions={0} | all-to-all | bytes 2359296 | tf_op jit(solution)/shard_map/all_to_all | solution.py:112
  216.3 5.7 %copy.41 = bf16[64,18,512]{0,1,2:T(8,128)(2,1)} copy(bf16[64,18,512]{2,1,0:T(8,128)(2,1)} %bitcast.94) | data formatting | bytes 2359296 | tf_op jit(solution)/shard_map/tile | solution.py:14
  222.0 8.1 %tile.12 = bf16[64,18,4,512]{0,1,3,2:T(8,128)(2,1)} broadcast(bf16[64,18,512]{0,1,2:T(8,128)(2,1)} %copy.41), dimensions={0,1,3} | broadcast | bytes 5898240 | tf_op jit(solution)/shard_map/tile | solution.py:14
  230.0 10.1 %reshape.87 = bf16[4,2,294912]{2,1,0:T(2,128)(2,1)} reshape(bf16[2048,1,18,64]{3,2,1,0:T(8,128)(2,1)} %bitcast.91) | data formatting | bytes 9437184
  240.2 58.6 %all_to_all.32 = bf16[4,2,294912]{2,1,0:T(2,128)(2,1)} all-to-all(bf16[4,2,294912]{2,1,0:T(2,128)(2,1)} %reshape.87), channel_id=1, replica_groups=mesh['grp'=2,'ep_0'=32,'ep_1'=2,'tp'=4] {'tp'}, dimensions={0} | all-to-all | bytes 9437184 | tf_op jit(solution)/shard_map/all_to_all | solution.py:14
  298.8 11.9 %reshape.88 = bf16[2048,1,18,64]{3,2,1,0:T(8,128)(2,1)} reshape(bf16[4,2,294912]{2,1,0:T(2,128)(2,1)} %all_to_all.32) | data formatting | bytes 9437184
  310.7 13.9 %copy.42 = bf16[64,1,18,2048]{3,0,2,1:T(8,128)(2,1)} copy(bf16[64,1,18,2048]{0,2,1,3:T(8,128)(2,1)} %bitcast.90) | data formatting | bytes 9437184 | tf_op jit(solution)/shard_map/all_to_all | solution.py:14
  324.6 3.9 fusion.9
  328.7 1.5 fusion.25
  330.5 28.5 %all_to_all.33 = bf16[4,64,1,18,256]{4,1,3,2,0:T(8,128)(2,1)S(1)} all-to-all(bf16[4,64,1,18,256]{4,1,3,2,0:T(8,128)(2,1)S(1)} %broadcast_in_dim.8), channel_id=1, replica_groups=mesh['grp'=2,'ep_0'=32,'ep_1'=2,'tp'=4] {'tp'}, dimensions={0} | all-to-all | bytes 4718592 | tf_op jit(solution)/shard_map/all_to_all | solution.py:19
  359.0 2.0 copy.43
  361.1 2.9 reshape.77
  364.0 3.0 fusion.8
  367.8 8.4 %all_to_all.34 = bf16[32,2,1,1,18,512]{5,0,4,3,2,1:T(8,128)(2,1)S(1)} all-to-all(bf16[32,2,1,1,18,512]{5,0,4,3,2,1:T(8,128)(2,1)S(1)} %copy.44), channel_id=1, replica_groups=mesh['grp'=2,'ep_0'=32,'ep_1'=2,'tp'=4] {'ep_1'}, dimensions={1} | all-to-all | bytes 2359296 | tf_op jit(solution)/shard_map/all_to_all | solution.py:50
  376.2 2.3 copy.45
  378.5 7.2 %all-to-all-start.5 = ((bf16[32,2,1,1,18,512]{5,1,4,3,2,0:T(2,128)(2,1)}), bf16[32,2,1,1,18,512]{5,1,4,3,2,0:T(2,128)(2,1)}, u32[]{:S(2)}, u32[]{:S(2)}) async-start(bf16[32,2,1,1,18,512]{5,1,4,3,2,0:T(2,128)(2,1)} %copy.45), calls=%async_computation.5 | async-start | bytes 2359296 | tf_op jit(solution)/shard_map/all_to_all | solution.py:50
  385.7 114.5 %all-to-all-done.5 = bf16[32,2,1,1,18,512]{5,1,4,3,2,0:T(2,128)(2,1)} async-done(((bf16[32,2,1,1,18,512]{5,1,4,3,2,0:T(2,128)(2,1)}), bf16[32,2,1,1,18,512]{5,1,4,3,2,0:T(2,128)(2,1)}, u32[]{:S(2)}, u32[]{:S(2)}) %all-to-all-start.5) | async-done | bytes 1179680 | tf_op jit(solution)/shard_map/all_to_all | solution.py:50
  500.2 1.6 copy.46
  503.0 2.1 fusion.23
  505.1 1.5 fusion.24
  (41 shorter events, 8.0 us)
Async XLA Ops:
  0.0 364.0 %copy-start = (bf16[1,1024,512]{2,1,0:T(8,128)(2,1)S(1)}, bf16[1,1024,512]{2,1,0:T(8,128)(2,1)}, u32[]{:S(2)}) copy-start(bf16[1,1024,512]{2,1,0:T(8,128)(2,1)} %param.17) | copy-start | bytes 3145732
  1.8 10.7 %all-to-all-start = ((f32[4,1,384]{2,1,0:T(1,128)}), f32[4,1,384]{2,1,0:T(1,128)S(1)}, u32[]{:S(2)}, u32[]{:S(2)}) async-start(f32[4,1,384]{2,1,0:T(1,128)} %broadcast_in_dim.6), calls=%async_computation | async-start | bytes 12288 | tf_op jit(solution)/shard_map/all_to_all | solution.py:19
  7.0 5.6 %copy-start.3 = (bf16[384,512]{1,0:T(8,128)(2,1)S(1)}, bf16[384,512]{1,0:T(8,128)(2,1)}, u32[]{:S(2)}) copy-start(bf16[384,512]{1,0:T(8,128)(2,1)} %param.9) | copy-start | bytes 1179652
  310.7 13.9 %copy-start.6 = (bf16[1,2048,256]{2,1,0:T(8,128)(2,1)S(1)}, bf16[1,2048,256]{2,1,0:T(8,128)(2,1)}, u32[]{:S(2)}) copy-start(bf16[1,2048,256]{2,1,0:T(8,128)(2,1)} %param.15) | copy-start | bytes 3145732
  324.6 3.9 copy-start.1
  324.6 4.1 copy-start.7
  378.5 7.2 %copy-start.4 = (f32[384,2]{0,1:T(2,128)S(1)}, f32[384,2]{0,1:T(2,128)}, u32[]{:S(2)}) copy-start(f32[384,2]{0,1:T(2,128)} %param.13) | copy-start | bytes 9220
  378.5 7.2 %copy-start.5 = (f32[384]{0:T(512)S(1)}, f32[384]{0:T(512)}, u32[]{:S(2)}) copy-start(f32[384]{0:T(512)} %param.12) | copy-start | bytes 4612
  378.5 121.8 %all-to-all-start.5 = ((bf16[32,2,1,1,18,512]{5,1,4,3,2,0:T(2,128)(2,1)}), bf16[32,2,1,1,18,512]{5,1,4,3,2,0:T(2,128)(2,1)}, u32[]{:S(2)}, u32[]{:S(2)}) async-start(bf16[32,2,1,1,18,512]{5,1,4,3,2,0:T(2,128)(2,1)} %copy.45), calls=%async_computation.5 | async-start | bytes 2359296 | tf_op jit(solution)/shard_map/all_to_all | solution.py:50
  503.0 2.1 copy-start.2
